TPU v7x, 32 devices: a whole 2x2x4 slice. The times are simulated.
32 devices in a mesh: ep: 4 (over y, x), tp: 8 (over z, core).
Axes of the slice: x: 2, y: 2, z: 4, core: 2. Of those that a mesh axis runs over, the one named last changes fastest.
Arguments:
- query_heads: bfloat16 [1024, 2048], P('ep', 'tp'), may hold values from -60 to 60
- key_heads: bfloat16 [1024, 2048], P('ep', 'tp'), may hold values from -40.5 to 40.5
- value_heads: bfloat16 [1024, 2048], P('ep', 'tp'), may hold values from -6 to 6
- diff_lambda: float32 [16], P('tp'), may hold values from 0.3 to 0.8
- sub_gain: float32 [128], replicated, may hold values from 0.1 to 1.9
- out_weight: bfloat16 [2048, 4096], P('tp'), may hold values from -0.125 to 0.125
- routed_input: bfloat16 [1024, 4096], P('ep', 'tp'), may hold values from -40 to 40
- routes: int32 [1024, 2], P('ep'), may hold values from 0 to 3, all different within a row; in each aligned block of 256 rows (0 to 255, 256 to 511, ...) at most 256 rows name the same one
- route_weights: float32 [1024, 2], P('ep'), may hold values from 0.3 to 1.5
- expert_gate: bfloat16 [4, 4096, 4096], P('ep', None, 'tp'), may hold values from -0.09375 to 0.09375
- expert_up: bfloat16 [4, 4096, 4096], P('ep', None, 'tp'), may hold values from -0.09375 to 0.09375
- expert_down: bfloat16 [4, 4096, 4096], P('ep', 'tp'), may hold values from -0.09375 to 0.09375
- shared_gate: bfloat16 [4096, 2048], P(None, 'tp'), may hold values from -0.09375 to 0.09375
- shared_up: bfloat16 [4096, 2048], P(None, 'tp'), may hold values from -0.09375 to 0.09375
- shared_down: bfloat16 [2048, 4096], P('tp'), may hold values from -0.125 to 0.125
Outputs:
- mixer_output: bfloat16 [1024, 4096], P('ep', 'tp')
- routed_output: bfloat16 [1024, 4096], P('ep', 'tp')
Inputs may be any that keep to these rules, and one draw needn't show every extreme that they name: `routes`: each row names 2 different experts. In each aligned block of 256 rows no expert is named by more than 256 rows, a bound that some block reaches.
All inputs are finite; a program needn't handle non-finite values.
Results may differ from a plain program's by a relative error of at most 0.02.
Values may be sent and summed in bfloat16 or wider, within the bound.
A program may use at most 128 MiB of HBM per device.

v0:
```python
import jax
import jax.numpy as jnp
from jax import lax
from jax.sharding import PartitionSpec as P

ROPE_BASE = 10000.0
NORM_EPS = 1e-06
MASKED = -1e30


def rotate(values, positions):
    half_width = values.shape[-1] // 2
    inverse_freq = ROPE_BASE ** (-jnp.arange(half_width, dtype=jnp.float32) / half_width)
    angles = positions.astype(jnp.float32)[:, None] * inverse_freq[None, :]
    angles = angles.reshape((angles.shape[0],) + (1,) * (values.ndim - 2) + (half_width,))
    cosine = jnp.cos(angles)
    sine_part = jnp.sin(angles)
    lower = values[..., :half_width]
    upper = values[..., half_width:]
    return jnp.concatenate(
        [lower * cosine - upper * sine_part, upper * cosine + lower * sine_part], axis=-1
    )


def mixer_terms(query_heads, key_heads, value_heads, diff_lambda, sub_gain, out_weight):
    row_count = query_heads.shape[0]
    local_heads = diff_lambda.shape[0]
    value_width = value_heads.shape[1] // local_heads
    key_width = query_heads.shape[1] // (2 * local_heads)
    score_scale = key_width ** (-0.5)
    offset = lax.axis_index("ep") * row_count
    positions = offset + jnp.arange(row_count, dtype=jnp.int32)
    last_row = offset + row_count - 1
    query_rot = rotate(
        query_heads.astype(jnp.float32).reshape(row_count, local_heads, 2, key_width), positions
    ).astype(jnp.bfloat16)
    queries = jnp.transpose(query_rot, (1, 2, 0, 3))
    key_rot = (
        rotate(
            key_heads.astype(jnp.float32).reshape(row_count, local_heads, 2, key_width), positions
        )
        .astype(jnp.bfloat16)
        .reshape(row_count, local_heads * 2 * key_width)
    )
    start_state = (
        jnp.full((local_heads, 2, row_count), MASKED, jnp.float32),
        jnp.zeros((local_heads, 2, row_count), jnp.float32),
        jnp.zeros((local_heads, 2, row_count, value_width), jnp.float32),
    )
    carried = start_state
    key_piece = lax.all_gather(key_rot, "ep", axis=0, tiled=True)
    value_piece = lax.all_gather(value_heads, "ep", axis=0, tiled=True)
    piece_rows = key_piece.shape[0]
    key_block = 512
    block_count = piece_rows // key_block
    key_blocks = key_piece.reshape(block_count, key_block, local_heads, 2, key_width)
    value_blocks = value_piece.reshape(block_count, key_block, local_heads, value_width)

    def block_step(running, block_item):
        key_rows, value_rows, block_index = block_item
        block_start = block_index * key_block

        def attend_block(partial_state):
            maxima, totals, weighted = partial_state
            key_positions = block_start + jnp.arange(key_block, dtype=jnp.int32)
            visible = key_positions[None, :] <= positions[:, None]
            scores = (
                jnp.einsum("hmqd,khmd->hmqk", queries, key_rows, preferred_element_type=jnp.float32)
                * score_scale
            )
            scores = jnp.where(visible, scores, MASKED)
            new_maxima = jnp.maximum(maxima, jnp.max(scores, axis=3))
            exp_weights = jnp.where(visible, jnp.exp(scores - new_maxima[..., None]), 0.0)
            shrink = jnp.exp(maxima - new_maxima)
            new_totals = totals * shrink + jnp.sum(exp_weights, axis=3)
            update = jnp.einsum(
                "hmqk,khw->hmqw",
                exp_weights.astype(jnp.bfloat16),
                value_rows,
                preferred_element_type=jnp.float32,
            )
            return (new_maxima, new_totals, weighted * shrink[..., None] + update)

        return (
            lax.cond(
                block_start <= last_row, attend_block, lambda partial_state: partial_state, running
            ),
            None,
        )

    carried, _ = lax.scan(
        block_step, carried, (key_blocks, value_blocks, jnp.arange(block_count, dtype=jnp.int32))
    )
    maxima, totals, weighted = carried
    attended = weighted / totals[..., None]
    mixed_heads = attended[:, 0] - diff_lambda[:, None, None] * attended[:, 1]
    normed = (
        mixed_heads
        * lax.rsqrt(jnp.mean(mixed_heads * mixed_heads, axis=2, keepdims=True) + NORM_EPS)
        * sub_gain
    )
    heads_out = jnp.transpose(normed.astype(jnp.bfloat16), (1, 0, 2)).reshape(
        row_count, local_heads * value_width
    )
    return jnp.dot(heads_out, out_weight, preferred_element_type=jnp.float32)


def expert_terms(
    routed_input, routes, expert_gate, expert_up, expert_down, shared_gate, shared_up, shared_down
):
    row_count, part_width = routed_input.shape
    top_count = routes.shape[1]
    local_experts = expert_gate.shape[0]
    groups = lax.axis_size("ep")
    experts = local_experts * groups
    capacity = 2 * row_count * top_count // experts
    copies = row_count * top_count
    flat_routes = routes.reshape(copies)
    onehot = (flat_routes[:, None] == jnp.arange(experts, dtype=jnp.int32)[None, :]).astype(
        jnp.int32
    )
    rank_within = jnp.sum((jnp.cumsum(onehot, axis=0) - onehot) * onehot, axis=1)
    slot_index = flat_routes * capacity + rank_within
    placer = (
        slot_index[:, None] == jnp.arange(experts * capacity, dtype=jnp.int32)[None, :]
    ).astype(jnp.bfloat16)
    token_slots = jnp.sum(placer.reshape(row_count, top_count, experts * capacity), axis=1)
    outgoing = jnp.dot(token_slots.T, routed_input, preferred_element_type=jnp.float32).astype(
        jnp.bfloat16
    )
    arrived = lax.all_to_all(
        outgoing.reshape(groups, local_experts * capacity, part_width),
        "ep",
        split_axis=0,
        concat_axis=0,
        tiled=True,
    )
    slot_count = groups * capacity
    slot_rows = jnp.transpose(
        arrived.reshape(groups, local_experts, capacity, part_width), (1, 0, 2, 3)
    ).reshape(local_experts, slot_count, part_width)
    slot_piece = lax.all_gather(slot_rows, "tp", axis=2, tiled=True)
    own_piece = lax.all_gather(routed_input[None], "tp", axis=2, tiled=True)
    own_rows = own_piece[0]
    gate_sum = jnp.einsum(
        "emc,ecf->emf", slot_piece, expert_gate, preferred_element_type=jnp.float32
    )
    up_sum = jnp.einsum("emc,ecf->emf", slot_piece, expert_up, preferred_element_type=jnp.float32)
    square_sum = jnp.sum(jnp.square(slot_piece.astype(jnp.float32)), axis=2)
    shared_gate_sum = jnp.dot(own_rows, shared_gate, preferred_element_type=jnp.float32)
    shared_up_sum = jnp.dot(own_rows, shared_up, preferred_element_type=jnp.float32)
    shared_square = jnp.sum(jnp.square(own_rows.astype(jnp.float32)), axis=1)
    full_width = expert_gate.shape[1]
    factor = lax.rsqrt(square_sum / full_width + NORM_EPS)[..., None]
    hidden = (jax.nn.silu(gate_sum * factor) * (up_sum * factor)).astype(jnp.bfloat16)
    shared_factor = lax.rsqrt(shared_square / full_width + NORM_EPS)[:, None]
    shared_hidden = (
        jax.nn.silu(shared_gate_sum * shared_factor) * (shared_up_sum * shared_factor)
    ).astype(jnp.bfloat16)
    shared_terms = jnp.dot(shared_hidden, shared_down, preferred_element_type=jnp.float32)
    routed_terms = jnp.einsum(
        "emf,efd->emd", hidden, expert_down, preferred_element_type=jnp.float32
    )
    routed_sum = lax.psum_scatter(
        routed_terms.astype(jnp.bfloat16), "tp", scatter_dimension=2, tiled=True
    ).astype(jnp.float32)
    return (routed_sum, shared_terms, placer)


def expert_finish(routed_sum, shared_sum, placer, route_weights):
    local_experts, slot_count, part_width = routed_sum.shape
    groups = lax.axis_size("ep")
    capacity = slot_count // groups
    leaving = jnp.transpose(
        routed_sum.astype(jnp.bfloat16).reshape(local_experts, groups, capacity, part_width),
        (1, 0, 2, 3),
    ).reshape(groups, local_experts * capacity, part_width)
    returned = lax.all_to_all(leaving, "ep", split_axis=0, concat_axis=0, tiled=True)
    copy_results = jnp.dot(
        placer,
        returned.reshape(groups * local_experts * capacity, part_width),
        preferred_element_type=jnp.float32,
    )
    row_count, top_count = route_weights.shape
    routed = jnp.sum(
        copy_results.reshape(row_count, top_count, part_width) * route_weights[:, :, None], axis=1
    )
    return (routed + shared_sum).astype(jnp.bfloat16)


def body(
    query_heads,
    key_heads,
    value_heads,
    diff_lambda,
    sub_gain,
    out_weight,
    routed_input,
    routes,
    route_weights,
    expert_gate,
    expert_up,
    expert_down,
    shared_gate,
    shared_up,
    shared_down,
):
    mixer_partial = mixer_terms(
        query_heads, key_heads, value_heads, diff_lambda, sub_gain, out_weight
    )
    routed_sum, shared_terms, placer = expert_terms(
        routed_input,
        routes,
        expert_gate,
        expert_up,
        expert_down,
        shared_gate,
        shared_up,
        shared_down,
    )
    mixer_sum, shared_sum = (
        lax.psum_scatter(
            mixer_partial.astype(jnp.bfloat16), "tp", scatter_dimension=1, tiled=True
        ).astype(jnp.float32),
        lax.psum_scatter(
            shared_terms.astype(jnp.bfloat16), "tp", scatter_dimension=1, tiled=True
        ).astype(jnp.float32),
    )
    return (
        mixer_sum.astype(jnp.bfloat16),
        expert_finish(routed_sum, shared_sum, placer, route_weights),
    )


def solution(mesh):
    placed = (
        P("ep", "tp"),
        P("ep", "tp"),
        P("ep", "tp"),
        P("tp"),
        P(),
        P("tp", None),
        P("ep", "tp"),
        P("ep", None),
        P("ep", None),
        P("ep", None, "tp"),
        P("ep", None, "tp"),
        P("ep", "tp", None),
        P(None, "tp"),
        P(None, "tp"),
        P("tp", None),
    )
    return jax.shard_map(
        body, mesh=mesh, in_specs=placed, out_specs=(P("ep", "tp"), P("ep", "tp")), check_vma=False
    )
```

profile of v0, /device:TPU:0, one launch (start us, length us, event | category | flops | bytes accessed | tf_op | source)
XLA Modules:
  0.0 315.3 jit_solution(10947524529678196263)
XLA Ops:
  7.2 0.9 copy.54
  8.5 1.2 reduce-window.6
  10.4 0.7 multiply_add_fusion.1
  11.4 1.4 convolution_convert_fusion.2
  12.8 19.2 %all_to_all.10 = bf16[4,256,512]{2,1,0:T(8,128)(2,1)} all-to-all(bf16[4,256,512]{2,1,0:T(8,128)(2,1)S(1)} %bitcast.120), channel_id=1, replica_groups=mesh['ep'=4,'tp'=8] {'ep'}, dimensions={0} | all-to-all | bytes 2097152 | tf_op jit(solution)/shard_map/all_to_all | solution.py:131
  32.1 0.7 all-gather.6.cloned.1.call-update
  32.9 81.1 %all-gather.4.cloned.1.call-done = bf16[1,1024,4096]{2,1,0:T(8,128)(2,1)} async-done(((bf16[1,1024,512]{2,1,0:T(8,128)(2,1)}), bf16[1,1024,4096]{2,1,0:T(8,128)(2,1)}) %all-gather.4.cloned.1.call-update) | async-done | bytes 8388624 | tf_op jit(solution)/shard_map/all_gather | solution.py:142
  114.0 5.2 %multiply_reduce_fusion = f32[1024]{0:T(1024)S(1)} fusion(bf16[1,1024,4096]{2,1,0:T(8,128)(2,1)} %all-gather.4.cloned.1.call-done), kind=kLoop, calls=%fused_computation.26 | loop fusion | flops 12581888 | bytes 8392704 | tf_op jit(solution)/shard_map/reduce_sum | solution.py:149
  119.8 8.1 %fusion.20 = f32[1024,512]{1,0:T(8,128)} fusion(bf16[1,1024,4096]{2,1,0:T(8,128)(2,1)S(1)} %copy-done.2, bf16[1,4096,512]{2,1,0:T(8,128)(2,1)} %param.29), kind=kOutput, calls=%fused_computation.27 | convolution fusion | flops 4294967296 | bytes 14680064 | tf_op jit(solution)/shard_map/emc,ecf->emf/dot_general | solution.py:148
  127.9 16.5 %convert_bitcast_fusion = bf16[1,1024,4096]{2,1,0:T(8,128)(2,1)} fusion(bf16[1,512,4096]{2,1,0:T(8,128)(2,1)} %param.30, f32[1024,512]{1,0:T(8,128)} %fusion.20, bf16[1,4096,512]{2,1,0:T(8,128)(2,1)} %param.28, bf16[1,1024,4096]{2,1,0:T(8,128)(2,1)} %all-gather.4.cloned.1.call-done, f32[1024]{0:T(1024)S(1)} %add_rsqrt_fusion), kind=kOutput, calls=%fused_computation.31 | convolution fusion | flops 8598323200 | bytes 27267072 | tf_op jit(solution)/shard_map/emf,efd->emd/dot_general | solution.py:161
  144.6 2.2 multiply_reduce_fusion.1
  146.9 2.3 convolution_multiply_fusion.1
  149.2 6.5 %convolution_convert_fusion = bf16[256,4096]{1,0:T(8,128)(2,1)} fusion(bf16[256,4096]{1,0:T(8,128)(2,1)S(1)} %copy-done, bf16[256,4096]{1,0:T(8,128)(2,1)} %all-gather.6.cloned.1.call-done, bf16[4096,256]{1,0:T(8,128)(2,1)} %param.32, f32[256,256]{1,0:T(8,128)S(1)} %convolution_multiply_fusion.1, f32[256]{0:T(256)S(1)} %add_rsqrt_fusion.2), kind=kOutput, calls=%fused_computation.32 | convolution fusion | flops 1075249152 | bytes 8651776 | tf_op jit(solution)/shard_map/dot_general | solution.py:160
  155.8 0.8 copy-done.5
  157.2 14.2 %all_gather.12 = bf16[1024,256]{0,1:T(8,128)(2,1)S(1)} all-gather(bf16[256,256]{0,1:T(8,128)(2,1)S(1)} %bitcast.127), channel_id=1, replica_groups=mesh['ep'=4,'tp'=8] {'ep'}, dimensions={0}, use_global_device_ids=true | all-gather | bytes 655360 | tf_op jit(solution)/shard_map/all_gather | solution.py:51
  171.8 10.2 %all_gather.13 = bf16[1024,256]{1,0:T(8,128)(2,1)S(1)} all-gather(bf16[256,256]{1,0:T(8,128)(2,1)S(1)} %copy-done.7), channel_id=1, replica_groups=mesh['ep'=4,'tp'=8] {'ep'}, dimensions={0}, use_global_device_ids=true | all-gather | bytes 655360 | tf_op jit(solution)/shard_map/all_gather | solution.py:52
  182.1 0.9 reshape.227
  183.0 1.9 copy.51
  185.0 4.9 %while.15 = (s32[]{:T(128)}, f32[2,2,256]{2,1,0:T(2,128)S(1)}, f32[2,2,256]{2,1,0:T(2,128)S(1)}, f32[2,2,256,128]{3,2,1,0:T(8,128)S(1)}, s32[2]{0:T(128)S(1)}, /...) while((s32[]{:T(128)}, f32[2,2,256]{2,1,0:T(2,128)S(1)}, ...), condition=%wide.region_5.6_spmd.clone, body=%wide.region_0.5_spmd.clone.sunk | while | flops 208538368 | bytes 10690895 | solution.py:91
  185.1 0.6 dynamic_slice.34
  186.3 2.3 conditional.3
  186.5 0.6 fusion.2
  187.6 1.0 convolution_add_fusion
  188.6 0.6 dynamic_slice.34
  190.8 0.9 copy-done.3
  191.7 2.0 convolution_convert_fusion.1
  193.8 40.7 %reduce-scatter.6.cloned.1.call-done = bf16[1,1024,512]{2,1,0:T(8,128)(2,1)} async-done(((bf16[1,1024,4096]{2,1,0:T(8,128)(2,1)}), bf16[1,1024,512]{2,1,0:T(8,128)(2,1)}) %reduce-scatter.6.cloned.1.call-update) | async-done | bytes 1048592 | tf_op jit(solution)/shard_map/reduce_scatter | solution.py:164
  234.5 16.0 %all_to_all.11 = bf16[4,256,512]{2,1,0:T(8,128)(2,1)S(1)} all-to-all(bf16[4,256,512]{2,1,0:T(8,128)(2,1)} %bitcast.122), channel_id=1, replica_groups=mesh['ep'=4,'tp'=8] {'ep'}, dimensions={0} | all-to-all | bytes 2097152 | tf_op jit(solution)/shard_map/all_to_all | solution.py:178
  250.5 0.8 fusion.42
  251.3 20.0 %reduce-scatter.8.cloned.1.call-done = bf16[256,512]{1,0:T(8,128)(2,1)} async-done(((bf16[256,4096]{1,0:T(8,128)(2,1)}), bf16[256,512]{1,0:T(8,128)(2,1)}) %reduce-scatter.8.cloned.1.call-update) | async-done | bytes 262160 | tf_op jit(solution)/shard_map/reduce_scatter | solution.py:225
  271.3 1.7 add_convert_fusion
  273.0 35.7 %reduce-scatter.4.cloned.1.call-done = bf16[256,512]{1,0:T(8,128)(2,1)} async-done(((bf16[256,4096]{1,0:T(8,128)(2,1)}), bf16[256,512]{1,0:T(8,128)(2,1)}) %reduce-scatter.4.cloned.1.call-update) | async-done | bytes 262160 | tf_op jit(solution)/shard_map/reduce_scatter | solution.py:222
  (72 shorter events, 4.9 us)
Async XLA Ops:
  7.2 142.0 %copy-start = (bf16[256,4096]{1,0:T(8,128)(2,1)S(1)}, bf16[256,4096]{1,0:T(8,128)(2,1)}, u32[]{:S(2)}) copy-start(bf16[256,4096]{1,0:T(8,128)(2,1)} %param.33) | copy-start | bytes 6291460
  7.2 106.8 %all-gather.4.cloned.1.call-start = ((), (), s32[]{:S(2)}) async-start(), calls=%async_computation.6 | async-start | bytes 9437184 | tf_op jit(solution)/shard_map/all_gather | solution.py:142
  32.1 112.5 %all-gather.6.cloned.1.call-start = ((), (), s32[]{:S(2)}) async-start(), calls=%async_computation.9 | async-start | bytes 2359296 | tf_op jit(solution)/shard_map/all_gather | solution.py:143
  32.8 201.7 %reduce-scatter.6.cloned.1.call-start = ((), (), s32[]{:S(2)}) async-start(), calls=%async_computation.7 | async-start | bytes 9437184 | tf_op jit(solution)/shard_map/reduce_scatter | solution.py:164
  114.0 5.8 %copy-start.2 = (bf16[1,1024,4096]{2,1,0:T(8,128)(2,1)S(1)}, bf16[1,1024,4096]{2,1,0:T(8,128)(2,1)}, u32[]{:S(2)}) copy-start(bf16[1,1024,4096]{2,1,0:T(8,128)(2,1)} %all-gather.4.cloned.1.call-done) | copy-start | bytes 25165828
  144.4 127.0 %reduce-scatter.8.cloned.1.call-start = ((), (), s32[]{:S(2)}) async-start(), calls=%async_computation.8 | async-start | bytes 2359296 | tf_op jit(solution)/shard_map/reduce_scatter | solution.py:225
  144.6 2.3 copy-start.1
  155.7 0.9 copy-start.5
  155.7 1.0 copy-start.6
  155.8 153.0 %reduce-scatter.4.cloned.1.call-start = ((), (), s32[]{:S(2)}) async-start(), calls=%async_computation.5 | async-start | bytes 2359296 | tf_op jit(solution)/shard_map/reduce_scatter | solution.py:222
  156.8 15.1 %copy-start.7 = (bf16[256,256]{1,0:T(8,128)(2,1)S(1)}, bf16[256,256]{1,0:T(8,128)(2,1)}, u32[]{:S(2)}) copy-start(bf16[256,256]{1,0:T(8,128)(2,1)} %param.21) | copy-start | bytes 393220
  186.5 1.1 copy-start.4
  189.9 0.7 copy-start.8
  189.9 0.8 copy-start.9
  190.1 1.6 copy-start.3
  193.8 56.8 %copy-start.10 = (f32[256,2]{0,1:T(2,128)S(1)}, f32[256,2]{0,1:T(2,128)}, u32[]{:S(2)}) copy-start(f32[256,2]{0,1:T(2,128)} %param.27) | copy-start | bytes 6148
Sparse Core Ops, SparseCore 0:
  32.2 81.7 all-gather.3
  115.6 27.6 all-gather.5
  145.6 88.8 reduce-scatter.5
  236.7 34.6 reduce-scatter.7
  274.0 34.6 reduce-scatter.3
where the time goes:
time: 316 us; the launch traced here: 315 us
  waiting for transfers between devices  178 us (56%)
  blocking collectives  59.7 us (19%)
  matrix products  39.2 us (12%)
  between operations  14.1 us (4%)
  other arithmetic  12.9 us (4%)
  local copies, waits for them, and re-layouts  9.29 us (3%)
    all_gather x1, waiting for transfers between devices, expert_terms(): slot_piece = lax.all_gather(slot_rows, 'tp', axis=2, tiled=True)  81.1 us
    reduce_scatter x1, waiting for transfers between devices, expert_terms(): lax.psum_scatter(routed_terms.astype(jnp.bfloat16), 'tp', scatter_dimensi...  40.7 us
    reduce_scatter x1, waiting for transfers between devices, body(): lax.psum_scatter(mixer_partial.astype(jnp.bfloat16), 'tp', scatter_dimens...  35.7 us
    reduce_scatter x1, waiting for transfers between devices, body(): lax.psum_scatter(shared_terms.astype(jnp.bfloat16), 'tp', scatter_dimensi...  20 us
    all_to_all x1, blocking collectives, expert_terms(): lax.all_to_all(outgoing.reshape(groups, local_experts * capacity, part_wi...  19.2 us
    dot_general x1, matrix products, expert_terms(): jnp.einsum('emf,efd->emd', hidden, expert_down, preferred_element_type=jn...  16.5 us
    all_to_all x1, blocking collectives, expert_finish(): lax.all_to_all(leaving, 'ep', split_axis=0, concat_axis=0, tiled=True)  16 us
    all_gather x1, blocking collectives, mixer_terms(): key_piece = lax.all_gather(key_rot, 'ep', axis=0, tiled=True)  14.2 us
  transfers between devices with their start and end apart: 5, of which 4 were waited for; matrix products, arithmetic and copies ran while one was open for 17% of the time, Pallas kernels for 0%

commit v1 on v0

--- a/solution.py
+++ b/solution.py
@@ -48,8 +48,11 @@
         jnp.zeros((local_heads, 2, row_count, value_width), jnp.float32),
     )
     carried = start_state
-    key_piece = lax.all_gather(key_rot, "ep", axis=0, tiled=True)
-    value_piece = lax.all_gather(value_heads, "ep", axis=0, tiled=True)
+    key_piece, value_piece = jnp.split(
+        lax.all_gather(jnp.concatenate([key_rot, value_heads], axis=1), "ep", axis=0, tiled=True),
+        [key_rot.shape[1]],
+        axis=1,
+    )
     piece_rows = key_piece.shape[0]
     key_block = 512
     block_count = piece_rows // key_block

time: 316 us -> 345 us (1.092)
  waiting for transfers between devices: 178 us -> 227 us
  blocking collectives: 59.7 us -> 35.4 us
  local copies, waits for them, and re-layouts: 9.29 us -> 13.1 us
    reduce_scatter x1, waiting for transfers between devices: 40.7 us -> 75 us  [expert_terms(): lax.psum_scatter(routed_terms.astype(jnp.bfloat16), 'tp', scatter_dimensi...]
    all_gather x2 -> x0, blocking collectives: 24.4 us -> none  [the longest x1 14.2 us: mixer_terms(): key_piece = lax.all_gather(key_rot, 'ep', axis=0, tiled=True)]
    all_gather x0 -> x1, waiting for transfers between devices: none -> 16.3 us  [mixer_terms(): lax.all_gather(jnp.concatenate([key_rot, value_heads], axis=1), 'ep', axi...]
  transfers between devices with their start and end apart: 5 -> 6, of which waited for: 4 -> 5; matrix products, arithmetic and copies ran while one was open for 17% -> 17% of each run, Pallas kernels for 0% -> 0%
where the time goes in v1:
time: 345 us; the launch traced here: 344 us
  waiting for transfers between devices  227 us (66%)
  matrix products  38.6 us (11%)
  blocking collectives  35.4 us (10%)
  between operations  14.4 us (4%)
  other arithmetic  13.7 us (4%)
  local copies, waits for them, and re-layouts  13.1 us (4%)
    all_gather x1, waiting for transfers between devices, expert_terms(): slot_piece = lax.all_gather(slot_rows, 'tp', axis=2, tiled=True)  79.6 us
    reduce_scatter x1, waiting for transfers between devices, expert_terms(): lax.psum_scatter(routed_terms.astype(jnp.bfloat16), 'tp', scatter_dimensi...  75 us
    reduce_scatter x1, waiting for transfers between devices, body(): lax.psum_scatter(mixer_partial.astype(jnp.bfloat16), 'tp', scatter_dimens...  35.6 us
    reduce_scatter x1, waiting for transfers between devices, body(): lax.psum_scatter(shared_terms.astype(jnp.bfloat16), 'tp', scatter_dimensi...  19.9 us
    all_to_all x1, blocking collectives, expert_terms(): lax.all_to_all(outgoing.reshape(groups, local_experts * capacity, part_wi...  19.4 us
    dot_general x1, matrix products, expert_terms(): jnp.einsum('emf,efd->emd', hidden, expert_down, preferred_element_type=jn...  16.4 us
    all_gather x1, waiting for transfers between devices, mixer_terms(): lax.all_gather(jnp.concatenate([key_rot, value_heads], axis=1), 'ep', axi...  16.3 us
    all_to_all x1, blocking collectives, expert_finish(): lax.all_to_all(leaving, 'ep', split_axis=0, concat_axis=0, tiled=True)  16 us
  transfers between devices with their start and end apart: 6, of which 5 were waited for; matrix products, arithmetic and copies ran while one was open for 17% of the time, Pallas kernels for 0%

profile of v1, /device:TPU:0, one launch (start us, length us, event | category | flops | bytes accessed | tf_op | source)
XLA Modules:
  0.0 344.4 jit_solution(6733491308956650615)
XLA Ops:
  7.2 0.9 copy.61
  8.5 1.2 reduce-window.6
  10.4 0.7 multiply_add_fusion.1
  11.4 1.4 convolution_convert_fusion.2
  12.8 19.4 %all_to_all.10 = bf16[4,256,512]{2,1,0:T(8,128)(2,1)} all-to-all(bf16[4,256,512]{2,1,0:T(8,128)(2,1)S(1)} %bitcast.118), channel_id=1, replica_groups=mesh['ep'=4,'tp'=8] {'ep'}, dimensions={0} | all-to-all | bytes 2097152 | tf_op jit(solution)/shard_map/all_to_all | solution.py:134
  32.3 0.7 all-gather.9.cloned.1.call-update
  33.7 0.7 pad_maximum_fusion
  34.5 79.6 %all-gather.7.cloned.1.call-done = bf16[1,1024,4096]{2,1,0:T(8,128)(2,1)} async-done(((bf16[1,1024,512]{2,1,0:T(8,128)(2,1)}), bf16[1,1024,4096]{2,1,0:T(8,128)(2,1)}) %all-gather.7.cloned.1.call-update) | async-done | bytes 8388624 | tf_op jit(solution)/shard_map/all_gather | solution.py:145
  114.2 5.2 %multiply_reduce_fusion = f32[1024]{0:T(1024)S(1)} fusion(bf16[1,1024,4096]{2,1,0:T(8,128)(2,1)} %all-gather.7.cloned.1.call-done), kind=kLoop, calls=%fused_computation.26 | loop fusion | flops 12581888 | bytes 8392704 | tf_op jit(solution)/shard_map/reduce_sum | solution.py:152
  119.9 8.1 %fusion.20 = f32[1024,512]{1,0:T(8,128)} fusion(bf16[1,1024,4096]{2,1,0:T(8,128)(2,1)S(1)} %copy-done.2, bf16[1,4096,512]{2,1,0:T(8,128)(2,1)} %param.29), kind=kOutput, calls=%fused_computation.27 | convolution fusion | flops 4294967296 | bytes 14680064 | tf_op jit(solution)/shard_map/emc,ecf->emf/dot_general | solution.py:151
  128.1 16.4 %convert_bitcast_fusion = bf16[1,1024,4096]{2,1,0:T(8,128)(2,1)} fusion(bf16[1,512,4096]{2,1,0:T(8,128)(2,1)} %param.30, f32[1024,512]{1,0:T(8,128)} %fusion.20, bf16[1,4096,512]{2,1,0:T(8,128)(2,1)} %param.28, bf16[1,1024,4096]{2,1,0:T(8,128)(2,1)} %all-gather.7.cloned.1.call-done, f32[1024]{0:T(1024)S(1)} %add_rsqrt_fusion), kind=kOutput, calls=%fused_computation.31 | convolution fusion | flops 8598323200 | bytes 27267072 | tf_op jit(solution)/shard_map/emf,efd->emd/dot_general | solution.py:164
  144.8 2.2 multiply_reduce_fusion.1
  147.1 2.3 convolution_multiply_fusion.1
  149.4 6.0 %convolution_convert_fusion = bf16[256,4096]{1,0:T(8,128)(2,1)} fusion(bf16[256,4096]{1,0:T(8,128)(2,1)S(1)} %copy-done, bf16[256,4096]{1,0:T(8,128)(2,1)} %all-gather.9.cloned.1.call-done, bf16[4096,256]{1,0:T(8,128)(2,1)} %param.32, f32[256,256]{1,0:T(8,128)S(1)} %convolution_multiply_fusion.1, f32[256]{0:T(256)S(1)} %add_rsqrt_fusion.2), kind=kOutput, calls=%fused_computation.32 | convolution fusion | flops 1075249152 | bytes 8651776 | tf_op jit(solution)/shard_map/dot_general | solution.py:163
  155.5 16.3 %all-gather.5.cloned.1.call-done = bf16[1024,512]{1,0:T(8,128)(2,1)} async-done(((bf16[256,512]{1,0:T(8,128)(2,1)}), bf16[1024,512]{1,0:T(8,128)(2,1)}) %all-gather.5.cloned.1.call-update) | async-done | bytes 1048592 | tf_op jit(solution)/shard_map/all_gather | solution.py:52
  171.8 2.1 fusion.66
  173.9 1.4 reshape.244
  175.3 2.4 copy.57
  177.6 1.2 reshape.227
  178.8 0.9 copy.58
  179.8 4.9 %while.15 = (s32[]{:T(128)}, f32[2,2,256]{2,1,0:T(2,128)S(1)}, f32[2,2,256]{2,1,0:T(2,128)S(1)}, f32[2,2,256,128]{3,2,1,0:T(8,128)S(1)}, s32[2]{0:T(128)S(1)}, /...) while((s32[]{:T(128)}, f32[2,2,256]{2,1,0:T(2,128)S(1)}, ...), condition=%wide.region_5.6_spmd.clone, body=%wide.region_0.5_spmd.clone.sunk | while | flops 208538368 | bytes 10690895 | solution.py:94
  179.8 0.6 dynamic_slice.34
  181.1 2.3 conditional.3
  182.4 1.0 convolution_add_fusion
  185.6 0.9 copy-done.3
  186.5 2.0 convolution_convert_fusion.1
  188.6 75.0 %reduce-scatter.6.cloned.1.call-done = bf16[1,1024,512]{2,1,0:T(8,128)(2,1)} async-done(((bf16[1,1024,4096]{2,1,0:T(8,128)(2,1)}), bf16[1,1024,512]{2,1,0:T(8,128)(2,1)}) %reduce-scatter.6.cloned.1.call-update) | async-done | bytes 1048592 | tf_op jit(solution)/shard_map/reduce_scatter | solution.py:167
  263.5 16.0 %all_to_all.11 = bf16[4,256,512]{2,1,0:T(8,128)(2,1)S(1)} all-to-all(bf16[4,256,512]{2,1,0:T(8,128)(2,1)} %bitcast.120), channel_id=1, replica_groups=mesh['ep'=4,'tp'=8] {'ep'}, dimensions={0} | all-to-all | bytes 2097152 | tf_op jit(solution)/shard_map/all_to_all | solution.py:181
  279.5 0.7 fusion.42
  280.3 19.9 %reduce-scatter.8.cloned.1.call-done = bf16[256,512]{1,0:T(8,128)(2,1)} async-done(((bf16[256,4096]{1,0:T(8,128)(2,1)}), bf16[256,512]{1,0:T(8,128)(2,1)}) %reduce-scatter.8.cloned.1.call-update) | async-done | bytes 262160 | tf_op jit(solution)/shard_map/reduce_scatter | solution.py:228
  300.2 1.7 add_convert_fusion
  301.9 35.6 %reduce-scatter.4.cloned.1.call-done = bf16[256,512]{1,0:T(8,128)(2,1)} async-done(((bf16[256,4096]{1,0:T(8,128)(2,1)}), bf16[256,512]{1,0:T(8,128)(2,1)}) %reduce-scatter.4.cloned.1.call-update) | async-done | bytes 262160 | tf_op jit(solution)/shard_map/reduce_scatter | solution.py:225
  (75 shorter events, 5.7 us)
Async XLA Ops:
  7.2 142.2 %copy-start = (bf16[256,4096]{1,0:T(8,128)(2,1)S(1)}, bf16[256,4096]{1,0:T(8,128)(2,1)}, u32[]{:S(2)}) copy-start(bf16[256,4096]{1,0:T(8,128)(2,1)} %param.33) | copy-start | bytes 6291460
  7.2 107.0 %all-gather.7.cloned.1.call-start = ((), (), s32[]{:S(2)}) async-start(), calls=%async_computation.7 | async-start | bytes 9437184 | tf_op jit(solution)/shard_map/all_gather | solution.py:145
  12.8 20.2 %copy-start.5 = (bf16[256,256]{1,0:T(8,128)(2,1)S(1)}, bf16[256,256]{1,0:T(8,128)(2,1)}, u32[]{:S(2)}) copy-start(bf16[256,256]{1,0:T(8,128)(2,1)} %param.20) | copy-start | bytes 393220
  12.8 20.3 %copy-start.6 = (bf16[256,256]{1,0:T(8,128)(2,1)S(1)}, bf16[256,256]{1,0:T(8,128)(2,1)}, u32[]{:S(2)}) copy-start(bf16[256,256]{1,0:T(8,128)(2,1)} %param.19) | copy-start | bytes 393220
  32.2 1.5 copy-start.7
  32.2 112.6 %all-gather.9.cloned.1.call-start = ((), (), s32[]{:S(2)}) async-start(), calls=%async_computation.10 | async-start | bytes 2359296 | tf_op jit(solution)/shard_map/all_gather | solution.py:146
  33.0 138.8 %all-gather.5.cloned.1.call-start = ((), (), s32[]{:S(2)}) async-start(), calls=%async_computation.5 | async-start | bytes 1310720 | tf_op jit(solution)/shard_map/all_gather | solution.py:52
  34.5 229.0 %reduce-scatter.6.cloned.1.call-start = ((), (), s32[]{:S(2)}) async-start(), calls=%async_computation.8 | async-start | bytes 9437184 | tf_op jit(solution)/shard_map/reduce_scatter | solution.py:167
  114.2 5.8 %copy-start.2 = (bf16[1,1024,4096]{2,1,0:T(8,128)(2,1)S(1)}, bf16[1,1024,4096]{2,1,0:T(8,128)(2,1)}, u32[]{:S(2)}) copy-start(bf16[1,1024,4096]{2,1,0:T(8,128)(2,1)} %all-gather.7.cloned.1.call-done) | copy-start | bytes 25165828
  144.5 155.6 %reduce-scatter.8.cloned.1.call-start = ((), (), s32[]{:S(2)}) async-start(), calls=%async_computation.9 | async-start | bytes 2359296 | tf_op jit(solution)/shard_map/reduce_scatter | solution.py:228
  144.8 2.3 copy-start.1
  155.4 182.1 %reduce-scatter.4.cloned.1.call-start = ((), (), s32[]{:S(2)}) async-start(), calls=%async_computation.6 | async-start | bytes 2359296 | tf_op jit(solution)/shard_map/reduce_scatter | solution.py:225
  181.2 1.1 copy-start.4
  184.7 0.7 copy-start.8
  184.7 0.8 copy-start.9
  184.9 1.6 copy-start.3
  188.5 91.0 %copy-start.10 = (f32[256,2]{0,1:T(2,128)S(1)}, f32[256,2]{0,1:T(2,128)}, u32[]{:S(2)}) copy-start(f32[256,2]{0,1:T(2,128)} %param.27) | copy-start | bytes 6148
Sparse Core Ops, SparseCore 0:
  32.4 81.7 all-gather.6
  115.8 27.6 all-gather.8
  145.9 25.8 all-gather.4
  173.9 89.5 reduce-scatter.5
  265.6 34.5 reduce-scatter.7
  302.9 34.5 reduce-scatter.3
